TPU v7x, 32 devices: a whole 2x2x4 slice. The times are simulated.
32 devices in a mesh: sp: 8 (over z, y), tp: 4 (over x, core).
Axes of the slice: x: 2, y: 2, z: 4, core: 2. Of those that a mesh axis runs over, the one named last changes fastest.
Arguments:
- out_cotangent: bfloat16 [1024, 2048], P('sp', 'tp'), may hold values from -6 to 6
- expert_input: bfloat16 [1024, 2048], P('sp', 'tp'), may hold values from -6 to 6
- routes: int32 [1024, 2], P('sp'), may hold values from 0 to 7, as said below
- route_weights: float32 [1024, 2], P('sp'), may hold values from 0.2 to 1
- gate_proj: bfloat16 [8, 2048, 3584], P('sp', None, 'tp'), may hold values from -0.125 to 0.125
- up_proj: bfloat16 [8, 2048, 3584], P('sp', None, 'tp'), may hold values from -0.125 to 0.125
- down_proj: bfloat16 [8, 3584, 2048], P('sp', 'tp'), may hold values from -0.09375 to 0.09375
- conv_out: bfloat16 [1024, 2048], P('sp', 'tp'), may hold values from -27 to 27
- conv_mean: float32 [1024], P('sp'), may hold values from -3 to 3
- conv_rstd: float32 [1024], P('sp'), may hold values from 0.25 to 1
- norm_gain: float32 [2048], P('tp'), may hold values from 0.1 to 1.9
- taps: float32 [31, 2048], P(None, 'tp'), may hold values from -1 to 1
- out_proj: bfloat16 [2048, 2048], P(None, 'tp'), may hold values from -0.125 to 0.125
Outputs:
- gate_grad: bfloat16 [8, 2048, 3584], P('sp', None, 'tp')
- up_grad: bfloat16 [8, 2048, 3584], P('sp', None, 'tp')
- down_grad: bfloat16 [8, 3584, 2048], P('sp', 'tp')
- proj_grad: float32 [2048, 2048], P('sp', 'tp')
- stream_grad: bfloat16 [1024, 2048], P('sp', 'tp')
- conv_in_grad: bfloat16 [1024, 2048], P('sp', 'tp')
Inputs may be any that keep to these rules, and one draw needn't show every extreme that they name: `routes`: each row names 2 different experts. In each aligned block of 128 rows (the rows of one device) no expert is named by more than 48 rows, and one expert, the same in every block, is named by exactly 48 rows of every block.
All inputs are finite; a program needn't handle non-finite values.
Results may differ from a plain program's by a relative error of at most 0.02.
Values may be sent and summed in bfloat16 or wider, within the bound.
A program may use at most 128 MiB of HBM per device.

v0:
```python
import jax
import jax.numpy as jnp
from jax import lax
from jax.sharding import PartitionSpec as P

OUTER_DIMS = (((0,), (0,)), ((), ()))
INNER_DIMS = (((1,), (1,)), ((), ()))


def passed_along(value, axis, steps):
    count = lax.axis_size(axis)
    leading, last = (max(0, -steps), min(count, count - steps))
    return lax.ppermute(value, axis, [(source, source + steps) for source in range(leading, last)])


def body(
    out_cotangent,
    expert_input,
    routes,
    route_weights,
    gate_proj,
    up_proj,
    down_proj,
    conv_out,
    conv_mean,
    conv_rstd,
    norm_gain,
    taps,
    out_proj,
):
    tok_rows, local_width = out_cotangent.shape
    experts = lax.axis_size("sp")
    width_parts = lax.axis_size("tp")
    capacity = 3 * tok_rows // experts
    per_token = routes.shape[1]
    assigned = routes.reshape(-1)
    pair_count = assigned.shape[0]
    onehot = (assigned[:, None] == jnp.arange(experts, dtype=jnp.int32)[None, :]).astype(jnp.int32)
    earlier = jnp.cumsum(onehot, axis=0) - onehot
    within_rank = jnp.sum(earlier * onehot, axis=1)
    slot_index = within_rank * experts + assigned
    source_pair = (
        jnp.full((capacity * experts,), pair_count, jnp.int32)
        .at[slot_index]
        .set(jnp.arange(pair_count, dtype=jnp.int32))
    )
    filled = source_pair < pair_count
    safe_pair = jnp.where(filled, source_pair, 0)
    token_index = safe_pair // per_token
    send_rows = jnp.where(filled[:, None], expert_input[token_index], jnp.zeros((), jnp.bfloat16))
    slot_weight = jnp.where(filled, route_weights.reshape(-1)[safe_pair], 0.0)
    send_cot = (slot_weight[:, None] * out_cotangent[token_index].astype(jnp.float32)).astype(
        jnp.bfloat16
    )
    send_rows = send_rows.reshape(capacity, experts, local_width)
    send_cot = send_cot.reshape(capacity, experts, local_width)
    rows_mid, cot_mid = (
        lax.all_to_all(send_rows, "sp", split_axis=1, concat_axis=1, tiled=True),
        lax.all_to_all(send_cot, "sp", split_axis=1, concat_axis=1, tiled=True),
    )
    rows_in, cot_in = (
        lax.all_gather(rows_mid, "tp", axis=2, tiled=True),
        lax.all_gather(cot_mid, "tp", axis=2, tiled=True),
    )
    full_width = local_width * width_parts
    rows_in = rows_in.reshape(capacity * experts, full_width)
    cot_in = cot_in.reshape(capacity * experts, full_width)
    gate_local = gate_proj[0]
    up_local = up_proj[0]
    down_local = down_proj[0]
    gate_pre = jnp.dot(rows_in, gate_local, preferred_element_type=jnp.float32)
    up_pre = jnp.dot(rows_in, up_local, preferred_element_type=jnp.float32)
    gate_sigmoid = jax.nn.sigmoid(gate_pre)
    activation = (gate_pre * gate_sigmoid * up_pre).astype(jnp.bfloat16)
    act_grad = lax.dot_general(cot_in, down_local, INNER_DIMS, preferred_element_type=jnp.float32)
    gate_back = (act_grad * up_pre * gate_sigmoid * (1.0 + gate_pre * (1.0 - gate_sigmoid))).astype(
        jnp.bfloat16
    )
    up_back = (act_grad * gate_pre * gate_sigmoid).astype(jnp.bfloat16)
    down_grad = lax.dot_general(
        activation, cot_in, OUTER_DIMS, preferred_element_type=jnp.float32
    ).astype(jnp.bfloat16)[None]
    gate_grad = lax.dot_general(
        rows_in, gate_back, OUTER_DIMS, preferred_element_type=jnp.float32
    ).astype(jnp.bfloat16)[None]
    up_grad = lax.dot_general(
        rows_in, up_back, OUTER_DIMS, preferred_element_type=jnp.float32
    ).astype(jnp.bfloat16)[None]
    partial_rows = lax.dot_general(
        gate_back, gate_local, INNER_DIMS, preferred_element_type=jnp.float32
    )
    partial_rows = partial_rows + lax.dot_general(
        up_back, up_local, INNER_DIMS, preferred_element_type=jnp.float32
    )
    block_rows = partial_rows.astype(jnp.bfloat16)
    summed = lax.psum_scatter(
        block_rows.reshape(capacity, experts, full_width), "tp", scatter_dimension=2, tiled=True
    ).astype(jnp.float32)
    routed = lax.all_to_all(
        summed.astype(jnp.bfloat16), "sp", split_axis=1, concat_axis=1, tiled=True
    )
    routed_flat = routed.reshape(capacity * experts, local_width)
    per_pair = routed_flat[slot_index].reshape(tok_rows, per_token, local_width)
    routed_sum = jnp.sum(per_pair, axis=1, dtype=jnp.float32)
    stream = (out_cotangent.astype(jnp.float32) + routed_sum).astype(jnp.bfloat16)
    stream_whole = lax.all_gather(stream, "tp", axis=1, tiled=True)
    normed = (conv_out.astype(jnp.float32) - conv_mean[:, None]) * conv_rstd[:, None]
    scaled = normed * norm_gain[None, :]
    scaled_sigmoid = jax.nn.sigmoid(scaled)
    swished = (scaled * scaled_sigmoid).astype(jnp.bfloat16)
    swished_grad = jnp.dot(stream_whole, out_proj, preferred_element_type=jnp.float32)
    scaled_grad = (
        swished_grad * scaled_sigmoid * (1.0 + scaled * (1.0 - scaled_sigmoid)) * norm_gain[None, :]
    )
    stat_sums = lax.psum(
        (jnp.sum(scaled_grad, axis=1), jnp.sum(scaled_grad * normed, axis=1)), "tp"
    )
    first_mean = stat_sums[0][:, None] / full_width
    second_mean = stat_sums[1][:, None] / full_width
    conv_grad = conv_rstd[:, None] * (scaled_grad - first_mean - normed * second_mean)
    proj_grad = lax.psum_scatter(
        lax.dot_general(
            stream_whole, swished, OUTER_DIMS, preferred_element_type=jnp.float32
        ).astype(jnp.bfloat16),
        "sp",
        scatter_dimension=0,
        tiled=True,
    ).astype(jnp.float32)
    halo_rows = taps.shape[0] - 1
    following = passed_along(conv_grad[:halo_rows].astype(jnp.bfloat16), "sp", -1).astype(
        jnp.float32
    )
    extended = jnp.concatenate([conv_grad, following], axis=0)
    conv_sum = jnp.zeros((tok_rows, local_width), jnp.float32)
    for offset in range(halo_rows + 1):
        conv_sum = conv_sum + taps[offset][None, :] * extended[offset : offset + tok_rows]
    return (gate_grad, up_grad, down_grad, proj_grad, stream, conv_sum.astype(jnp.bfloat16))


def solution(mesh):
    in_specs = (
        P("sp", "tp"),
        P("sp", "tp"),
        P("sp", None),
        P("sp", None),
        P("sp", None, "tp"),
        P("sp", None, "tp"),
        P("sp", "tp", None),
        P("sp", "tp"),
        P("sp"),
        P("sp"),
        P("tp"),
        P(None, "tp"),
        P(None, "tp"),
    )
    out_specs = (
        P("sp", None, "tp"),
        P("sp", None, "tp"),
        P("sp", "tp", None),
        P("sp", "tp"),
        P("sp", "tp"),
        P("sp", "tp"),
    )
    return jax.shard_map(body, mesh=mesh, in_specs=in_specs, out_specs=out_specs, check_vma=False)
```

profile of v0, /device:TPU:0, one launch (start us, length us, event | category | flops | bytes accessed | tf_op | source)
XLA Modules:
  0.0 218.2 jit_solution(8300070704669556033)
XLA Ops:
  7.2 0.9 copy.33
  8.2 0.1 reshape.104
  8.3 0.1 eq.29
  8.5 0.1 eq.25
  8.6 0.6 reduce-window.6
  9.2 0.2 slice_reduce_fusion
  9.6 1.4 scatter_custom_fusion
  11.0 0.1 broadcast_in_dim.50
  11.2 2.1 gather_fusion
  13.3 0.1 copy_select_fusion
  13.4 19.2 %all_to_all.15 = bf16[48,8,512]{2,0,1:T(8,128)(2,1)S(1)} all-to-all(bf16[48,8,512]{2,0,1:T(8,128)(2,1)S(1)} %copy_select_fusion), channel_id=1, replica_groups=mesh['sp'=8,'tp'=4] {'sp'}, dimensions={1} | all-to-all | bytes 786432 | tf_op jit(solution)/shard_map/all_to_all | solution.py:58
  32.6 1.0 copy.38
  33.7 0.1 copy.39
  33.8 0.1 reshape.106
  33.9 2.8 %gather_fusion.1 = f32[384]{0:T(512)S(1)} fusion(f32[256]{0:T(256)S(1)} %reshape.106, s32[1024]{0:T(1024)S(1)} %pad_clamp_fusion.1), kind=kCustom, calls=%fused_computation.1 | custom fusion | bytes 4608 | tf_op jit(solution)/shard_map/gather | solution.py:51
  36.9 2.1 gather_fusion.2
  39.1 0.5 fusion.23
  39.5 15.0 %all_to_all.16 = bf16[48,8,512]{2,0,1:T(8,128)(2,1)S(1)} all-to-all(bf16[48,8,512]{2,0,1:T(8,128)(2,1)S(1)} %fusion.23), channel_id=1, replica_groups=mesh['sp'=8,'tp'=4] {'sp'}, dimensions={1} | all-to-all | bytes 786432 | tf_op jit(solution)/shard_map/all_to_all | solution.py:59
  54.5 1.0 copy.42
  55.5 0.2 reduce-scatter.3.cloned.1.call-start
  55.8 5.5 %fusion.2 = f32[384,896]{1,0:T(8,128)} fusion(bf16[1,2048,896]{2,1,0:T(8,128)(2,1)} %param.17, bf16[48,8,2048]{2,1,0:T(8,128)(2,1)} %all-gather.3.cloned.1.call-done), kind=kOutput, calls=%fused_computation.7 | convolution fusion | flops 1409286144 | bytes 6619136 | tf_op jit(solution)/shard_map/dot_general | solution.py:71
  61.3 2.9 %fusion.6 = f32[384,896]{1,0:T(8,128)} fusion(bf16[1,2048,896]{2,1,0:T(8,128)(2,1)S(1)} %copy-done.11, bf16[48,8,2048]{2,1,0:T(8,128)(2,1)S(1)} %copy-done.13), kind=kOutput, calls=%fused_computation.11 | convolution fusion | flops 1409286144 | bytes 6619136 | tf_op jit(solution)/shard_map/dot_general | solution.py:72
  64.2 9.7 %all-gather.5.cloned.1.call-done = bf16[48,8,2048]{2,1,0:T(8,128)(2,1)} async-done(((bf16[48,8,512]{2,1,0:T(8,128)(2,1)}), bf16[48,8,2048]{2,1,0:T(8,128)(2,1)}) %all-gather.5.cloned.1.call-update) | async-done | bytes 1572880 | tf_op jit(solution)/shard_map/all_gather | solution.py:63
  73.9 5.5 %multiply_convert_fusion.1 = (bf16[384,896]{1,0:T(8,128)(2,1)S(1)}, bf16[384,896]{1,0:T(8,128)(2,1)S(1)}) fusion(f32[384,896]{1,0:T(8,128)} %fusion.2, f32[384,896]{1,0:T(8,128)} %fusion.6, bf16[1,896,2048]{2,1,0:T(8,128)(2,1)} %param.19, bf16[48,8,2048]{2,1,0:T(8,128)(2,1)} %all-gather.5.cloned.1.call-done), kind=kOutput, calls=%fused_computation.57 | convolution fusion | flops 1413758976 | bytes 9371648 | tf_op jit(solution)/shard_map/dot_general | solution.py:75
  79.5 1.8 fusion
  81.4 0.7 copy-done.12
  82.0 1.8 fusion.12
  83.9 2.0 copy.43
  85.9 28.2 %reduce-scatter.3.cloned.1.call-done = bf16[48,8,512]{2,0,1:T(8,128)(2,1)} async-done(((bf16[48,8,2048]{2,0,1:T(8,128)(2,1)}), bf16[48,8,512]{2,0,1:T(8,128)(2,1)}) %reduce-scatter.3.cloned.1.call-update) | async-done | bytes 393232 | tf_op jit(solution)/shard_map/reduce_scatter | solution.py:96
  114.1 5.5 %all-to-all-start.2 = ((bf16[48,8,512]{2,0,1:T(8,128)(2,1)}), bf16[48,8,512]{2,0,1:T(8,128)(2,1)S(1)}, u32[]{:S(2)}, u32[]{:S(2)}) async-start(bf16[48,8,512]{2,0,1:T(8,128)(2,1)} %reduce-scatter.3.cloned.1.call-done), calls=%async_computation.3 | async-start | bytes 786432 | tf_op jit(solution)/shard_map/all_to_all | solution.py:99
  119.6 11.5 %all-to-all-done.2 = bf16[48,8,512]{2,0,1:T(8,128)(2,1)S(1)} async-done(((bf16[48,8,512]{2,0,1:T(8,128)(2,1)}), bf16[48,8,512]{2,0,1:T(8,128)(2,1)S(1)}, u32[]{:S(2)}, u32[]{:S(2)}) %all-to-all-start.2) | async-done | bytes 393248 | tf_op jit(solution)/shard_map/all_to_all | solution.py:99
  131.1 0.2 copy.50
  131.4 1.2 gather_fusion.3
  132.6 0.3 reshape.111
  132.9 0.6 reduce_sum.37
  133.6 6.7 %all_gather.11 = bf16[128,2048]{1,0:T(8,128)(2,1)S(1)} all-gather(bf16[128,512]{1,0:T(8,128)(2,1)S(1)} %add_convert_fusion.1), channel_id=1, replica_groups=mesh['sp'=8,'tp'=4] {'tp'}, dimensions={1}, use_global_device_ids=true | all-gather | bytes 655360 | tf_op jit(solution)/shard_map/all_gather | solution.py:106
  140.3 2.2 convolution_convert_fusion
  142.5 0.8 copy-done.5
  143.4 5.8 %convert_bitcast_fusion.1 = bf16[1,2048,896]{2,1,0:T(8,128)(2,1)} fusion(bf16[384,896]{1,0:T(8,128)(2,1)} %copy-done.18, bf16[48,8,2048]{2,1,0:T(8,128)(2,1)} %all-gather.3.cloned.1.call-done), kind=kOutput, calls=%fused_computation.16 | convolution fusion | flops 1411121152 | bytes 5931008 | tf_op jit(solution)/shard_map/dot_general | solution.py:86
  149.3 4.0 %convert_bitcast_fusion = bf16[1,896,2048]{2,1,0:T(8,128)(2,1)} fusion(bf16[48,8,2048]{2,1,0:T(8,128)(2,1)S(1)} %copy-done.14, f32[384,896]{1,0:T(8,128)S(1)} %copy-done.17, f32[384,896]{1,0:T(8,128)S(1)} %copy-done.16), kind=kOutput, calls=%fused_computation.15 | convolution fusion | flops 1413185536 | bytes 7995392 | tf_op jit(solution)/shard_map/dot_general | solution.py:80
  153.3 0.6 fusion.129
  153.9 7.1 %all-reduce = (f32[128]{0:T(128)S(1)}, f32[128]{0:T(128)S(1)}) all-reduce(f32[128]{0:T(128)S(1)} %get-tuple-element.7, f32[128]{0:T(128)S(1)} %get-tuple-element.6), channel_id=1, replica_groups=mesh['sp'=8,'tp'=4] {'tp'}, use_global_device_ids=true, to_apply=%region_10.11 | all-reduce | flops 256 | bytes 2048 | tf_op jit(solution)/shard_map/psum | solution.py:115
  161.0 0.1 subtract_multiply_fusion
  161.1 1.3 collective-permute-start
  162.4 5.7 %convert_bitcast_fusion.2 = bf16[1,2048,896]{2,1,0:T(8,128)(2,1)} fusion(bf16[384,896]{1,0:T(8,128)(2,1)} %copy-done.15, bf16[48,8,2048]{2,1,0:T(8,128)(2,1)} %all-gather.3.cloned.1.call-done), kind=kOutput, calls=%fused_computation.17 | convolution fusion | flops 1411121152 | bytes 5931008 | tf_op jit(solution)/shard_map/dot_general | solution.py:83
  168.2 2.0 fusion.29
  170.2 39.7 %reduce-scatter.5.cloned.1.call-done = bf16[256,512]{1,0:T(8,128)(2,1)} async-done(((bf16[2048,512]{1,0:T(8,128)(2,1)}), bf16[256,512]{1,0:T(8,128)(2,1)}) %reduce-scatter.5.cloned.1.call-update) | async-done | bytes 262160 | tf_op jit(solution)/shard_map/reduce_scatter | solution.py:121
  209.8 1.8 convert_element_type.91
  (68 shorter events, 0.9 us)
Async XLA Ops:
  7.2 146.1 %copy-start = (bf16[2048,512]{1,0:T(8,128)(2,1)S(1)}, bf16[2048,512]{1,0:T(8,128)(2,1)}, u32[]{:S(2)}) copy-start(bf16[2048,512]{1,0:T(8,128)(2,1)} %param.25) | copy-start | bytes 6291460
  7.2 4.0 %copy-start.2 = (bf16[128,512]{1,0:T(8,128)(2,1)S(1)}, bf16[128,512]{1,0:T(8,128)(2,1)}, u32[]{:S(2)}) copy-start(bf16[128,512]{1,0:T(8,128)(2,1)} %param.14) | copy-start | bytes 393220
  7.2 48.6 %all-gather.3.cloned.1.call-start = ((), (), s32[]{:S(2)}) async-start(), calls=%async_computation.5 | async-start | bytes 1966080 | tf_op jit(solution)/shard_map/all_gather | solution.py:62
  13.3 20.4 %copy-start.9 = (f32[128,2]{0,1:T(2,128)S(1)}, f32[128,2]{0,1:T(2,128)}, u32[]{:S(2)}) copy-start(f32[128,2]{0,1:T(2,128)} %param.16) | copy-start | bytes 3076
  32.6 4.3 %copy-start.1 = (bf16[128,512]{1,0:T(8,128)(2,1)S(1)}, bf16[128,512]{1,0:T(8,128)(2,1)}, u32[]{:S(2)}) copy-start(bf16[128,512]{1,0:T(8,128)(2,1)} %param.13) | copy-start | bytes 393220
  33.6 40.3 %all-gather.5.cloned.1.call-start = ((), (), s32[]{:S(2)}) async-start(), calls=%async_computation.6 | async-start | bytes 1966080 | tf_op jit(solution)/shard_map/all_gather | solution.py:63
  55.5 58.6 %reduce-scatter.3.cloned.1.call-start = ((), (), s32[]{:S(2)}) async-start(), calls=%async_computation.7 | async-start | bytes 1966080 | tf_op jit(solution)/shard_map/reduce_scatter | solution.py:96
  55.8 5.6 %copy-start.11 = (bf16[1,2048,896]{2,1,0:T(8,128)(2,1)S(1)}, bf16[1,2048,896]{2,1,0:T(8,128)(2,1)}, u32[]{:S(2)}) copy-start(bf16[1,2048,896]{2,1,0:T(8,128)(2,1)} %param.18) | copy-start | bytes 11010052
  55.8 5.5 %copy-start.13 = (bf16[48,8,2048]{2,1,0:T(8,128)(2,1)S(1)}, bf16[48,8,2048]{2,1,0:T(8,128)(2,1)}, u32[]{:S(2)}) copy-start(bf16[48,8,2048]{2,1,0:T(8,128)(2,1)} %all-gather.3.cloned.1.call-done) | copy-start | bytes 4718596
  73.9 5.6 %copy-start.10 = (bf16[1,2048,896]{2,1,0:T(8,128)(2,1)S(1)}, bf16[1,2048,896]{2,1,0:T(8,128)(2,1)}, u32[]{:S(2)}) copy-start(bf16[1,2048,896]{2,1,0:T(8,128)(2,1)} %param.17) | copy-start | bytes 11010052
  79.5 1.9 copy-start.15
  79.5 1.9 copy-start.18
  79.5 2.5 %copy-start.12 = (bf16[1,2048,896]{2,1,0:T(8,128)(2,1)S(1)}, bf16[1,2048,896]{2,1,0:T(8,128)(2,1)}, u32[]{:S(2)}) copy-start(bf16[1,2048,896]{2,1,0:T(8,128)(2,1)} %param.18) | copy-start | bytes 11010052
  114.1 17.1 %all-to-all-start.2 = ((bf16[48,8,512]{2,0,1:T(8,128)(2,1)}), bf16[48,8,512]{2,0,1:T(8,128)(2,1)S(1)}, u32[]{:S(2)}, u32[]{:S(2)}) async-start(bf16[48,8,512]{2,0,1:T(8,128)(2,1)} %reduce-scatter.3.cloned.1.call-done), calls=%async_computation.3 | async-start | bytes 786432 | tf_op jit(solution)/shard_map/all_to_all | solution.py:99
  119.6 90.2 %reduce-scatter.5.cloned.1.call-start = ((), (), s32[]{:S(2)}) async-start(), calls=%async_computation.8 | async-start | bytes 2359296 | tf_op jit(solution)/shard_map/reduce_scatter | solution.py:121
  132.5 7.8 %copy-start.3 = (bf16[128,512]{1,0:T(8,128)(2,1)S(1)}, bf16[128,512]{1,0:T(8,128)(2,1)}, u32[]{:S(2)}) copy-start(bf16[128,512]{1,0:T(8,128)(2,1)} %param.20) | copy-start | bytes 393220
  132.5 7.8 %copy-start.6 = (f32[128]{0:T(128)S(1)}, f32[128]{0:T(128)}, u32[]{:S(2)}) copy-start(f32[128]{0:T(128)} %param.22) | copy-start | bytes 1540
  132.5 7.8 %copy-start.7 = (f32[128]{0:T(128)S(1)}, f32[128]{0:T(128)}, u32[]{:S(2)}) copy-start(f32[128]{0:T(128)} %param.21) | copy-start | bytes 1540
  132.6 7.8 %copy-start.8 = (f32[512]{0:T(512)S(1)}, f32[512]{0:T(512)}, u32[]{:S(2)}) copy-start(f32[512]{0:T(512)} %param.23) | copy-start | bytes 6148
  133.6 8.9 %copy-start.4 = (bf16[128,512]{1,0:T(8,128)(2,1)}, bf16[128,512]{1,0:T(8,128)(2,1)S(1)}, u32[]{:S(2)}) copy-start(bf16[128,512]{1,0:T(8,128)(2,1)S(1)} %add_convert_fusion.1) | copy-start | bytes 393220
  142.5 0.8 copy-start.5
  143.4 5.9 %copy-start.14 = (bf16[48,8,2048]{2,1,0:T(8,128)(2,1)S(1)}, bf16[48,8,2048]{2,1,0:T(8,128)(2,1)}, u32[]{:S(2)}) copy-start(bf16[48,8,2048]{2,1,0:T(8,128)(2,1)} %all-gather.5.cloned.1.call-done) | copy-start | bytes 4718596
  143.4 5.8 %copy-start.16 = (f32[384,896]{1,0:T(8,128)S(1)}, f32[384,896]{1,0:T(8,128)}, u32[]{:S(2)}) copy-start(f32[384,896]{1,0:T(8,128)} %fusion.2) | copy-start | bytes 4128772
  143.4 5.8 %copy-start.17 = (f32[384,896]{1,0:T(8,128)S(1)}, f32[384,896]{1,0:T(8,128)}, u32[]{:S(2)}) copy-start(f32[384,896]{1,0:T(8,128)} %fusion.6) | copy-start | bytes 4128772
  161.1 7.0 %collective-permute-start = (bf16[30,512]{1,0:T(8,128)(2,1)S(1)}, bf16[30,512]{1,0:T(8,128)(2,1)S(1)}, u32[]{:S(2)}, u32[]{:S(2)}) collective-permute-start(bf16[30,512]{1,0:T(8,128)(2,1)S(1)} %slice.721), channel_id=1, source_target_pairs={{4,0},{8,4},{12,8},{16,12},{20,16},{24,20},{28,24},{5,1},{9,5},{13... | collective-permute-start | bytes 92168 | tf_op jit(solution)/shard_map/ppermute | solution.py:13
Sparse Core Ops, SparseCore 0:
  33.7 18.2 all-gather.2
  55.6 18.2 all-gather.4
  86.0 28.0 reduce-scatter.2
  142.7 67.1 reduce-scatter.4
where the time goes:
time: 219 us; the launch traced here: 218 us
  waiting for transfers between devices  89.1 us (41%)
  blocking collectives  48 us (22%)
  matrix products  36 us (16%)
  local copies, waits for them, and re-layouts  17.8 us (8%)
  between operations  14.2 us (6%)
  starting transfers between devices  7.15 us (3%)
  other arithmetic  6.03 us (3%)
    reduce_scatter x1, waiting for transfers between devices, body(): lax.psum_scatter(lax.dot_general(stream_whole, swished, OUTER_DIMS, prefe...  39.7 us
    reduce_scatter x1, waiting for transfers between devices, body(): lax.psum_scatter(block_rows.reshape(capacity, experts, full_width), 'tp',...  28.2 us
    all_to_all x1, blocking collectives, body(): lax.all_to_all(send_rows, 'sp', split_axis=1, concat_axis=1, tiled=True)  19.2 us
    all_to_all x1, blocking collectives, body(): lax.all_to_all(send_cot, 'sp', split_axis=1, concat_axis=1, tiled=True)  15 us
    all_to_all x1, waiting for transfers between devices, body(): lax.all_to_all(summed.astype(jnp.bfloat16), 'sp', split_axis=1, concat_ax...  11.5 us
    all_gather x1, waiting for transfers between devices, body(): lax.all_gather(cot_mid, 'tp', axis=2, tiled=True)  9.68 us
    psum x1, blocking collectives, body(): lax.psum((jnp.sum(scaled_grad, axis=1), jnp.sum(scaled_grad * normed, axi...  7.09 us
    all_gather x1, blocking collectives, body(): stream_whole = lax.all_gather(stream, 'tp', axis=1, tiled=True)  6.72 us
  transfers between devices with their start and end apart: 6, of which 4 were waited for; matrix products, arithmetic and copies ran while one was open for 15% of the time, Pallas kernels for 0%

commit v1 on v0

v1 whole, which is shorter than its diff:
```python
import functools

import jax
import jax.numpy as jnp
from jax import lax
from jax.experimental import pallas as pl
from jax.experimental.pallas import tpu as pltpu
from jax.sharding import PartitionSpec as P

OUTER_DIMS = (((0,), (0,)), ((), ()))
INNER_DIMS = (((1,), (1,)), ((), ()))
MESH = pl.DeviceIdType.MESH
VMEM = pltpu.VMEM


def flipped(index, bit):
    return index + bit - 2 * bit * ((index // bit) % 2)


def bits_of(count):
    bits, bit = [], 1
    while bit < count:
        bits.append(bit)
        bit *= 2
    return bits


def greet(devices):
    barrier = pltpu.get_barrier_semaphore()
    for device in devices:
        pl.semaphore_signal(barrier, inc=1, device_id=device, device_id_type=MESH)
    pl.semaphore_wait(barrier, len(devices))


def remote(src, dst, send_sem, recv_sem, device):
    return pltpu.make_async_remote_copy(
        src_ref=src, dst_ref=dst, send_sem=send_sem, recv_sem=recv_sem,
        device_id=device, device_id_type=MESH,
    )


def dispatch_kernel(
    experts, parts, send_ref, swished_ref, full_ref, gathered_ref,
    out_send, out_recv, sw_send, sw_recv, hop_send, hop_recv, local_sem,
):
    me, col = lax.axis_index("sp"), lax.axis_index("tp")
    width = send_ref.shape[3]
    bits = bits_of(parts)[::-1]
    greet(
        [(lax.rem(me + k, experts), col) for k in range(1, experts)]
        + [(me, flipped(col, bit)) for bit in bits]
    )

    def place(source, column):
        return full_ref.at[:, source, :, pl.ds(pl.multiple_of(column * width, width), width)]

    own = pltpu.make_async_copy(send_ref.at[me], place(me, col), local_sem.at[0])
    own.start()
    own_sw = pltpu.make_async_copy(swished_ref, gathered_ref.at[me], local_sem.at[1])
    own_sw.start()

    def out_copy(peer, slot):
        return remote(send_ref.at[peer], place(me, col), out_send.at[peer], out_recv.at[me], (peer, col))

    def sw_copy(peer):
        return remote(swished_ref, gathered_ref.at[me], sw_send.at[peer], sw_recv.at[me], (peer, col))

    def start_out(k, carry):
        out_copy(lax.rem(me + k, experts), k).start()
        return carry

    def start_sw(k, carry):
        sw_copy(lax.rem(me + k, experts)).start()
        return carry

    lax.fori_loop(1, experts, start_out, 0)
    lax.fori_loop(1, experts, start_sw, 0)
    own.wait()

    held = [[col]]
    for bit in bits:
        held.append(held[-1] + [flipped(column, bit) for column in held[-1]])
    starts, total = [], 0
    for level in range(len(bits)):
        starts.append(total)
        total += len(held[level])

    def hop(level, slot, column, source):
        index = starts[level] + slot
        return remote(
            place(source, column), place(source, column),
            hop_send.at[index, source], hop_recv.at[index, source],
            (me, flipped(col, bits[level])),
        )

    def hop_arrival(level, slot, source):
        index = starts[level] + slot
        column = flipped(held[level][slot], bits[level])
        return remote(
            place(source, column), place(source, column),
            hop_send.at[index, source], hop_recv.at[index, source],
            (me, flipped(col, bits[level])),
        )

    def advance(k, carry):
        source = lax.rem(me - k + experts, experts)

        @pl.when((k > 0) & (k < experts))
        def _():
            remote(
                send_ref.at[source], place(source, col), out_send.at[source],
                out_recv.at[source], (source, col),
            ).wait_recv()

        @pl.when(k < experts)
        def _():
            for level in range(len(bits)):
                hop(level, 0, col, source).start()

        for level in range(1, len(bits)):
            late = lax.rem(me - k + level + 2 * experts, experts)

            @pl.when((k >= level) & (k < experts + level))
            def _(level=level, late=late):
                size = len(held[level - 1])
                for slot in range(size):
                    hop_arrival(level - 1, slot, late).wait_recv()
                for later in range(level, len(bits)):
                    for slot in range(size, 2 * size):
                        hop(later, slot, held[level][slot], late).start()

        return carry

    lax.fori_loop(0, experts + len(bits) - 1, advance, 0)

    def finish(k, carry):
        source = lax.rem(me + k, experts)
        last = len(bits) - 1
        for slot in range(len(held[last])):
            hop_arrival(last, slot, source).wait_recv()
        for level in range(len(bits)):
            for slot in range(len(held[level])):
                hop(level, slot, held[level][slot], source).wait_send()

        @pl.when(k > 0)
        def _():
            out_copy(source, k).wait_send()
            sw_copy(source).wait_send()
            remote(
                swished_ref, gathered_ref.at[source], sw_send.at[source],
                sw_recv.at[source], (source, col),
            ).wait_recv()

        return carry

    lax.fori_loop(0, experts, finish, 0)
    own_sw.wait()


def dispatch(send, swished, experts, parts):
    _, _, capacity, width = send.shape
    hops = parts - 1
    return pl.pallas_call(
        functools.partial(dispatch_kernel, experts, parts),
        out_shape=(
            jax.ShapeDtypeStruct((2, experts, capacity, width * parts), jnp.bfloat16),
            jax.ShapeDtypeStruct((experts,) + swished.shape, jnp.bfloat16),
        ),
        in_specs=[pl.BlockSpec(memory_space=VMEM)] * 2,
        out_specs=[pl.BlockSpec(memory_space=VMEM)] * 2,
        scratch_shapes=[pltpu.SemaphoreType.DMA((experts,))] * 4
        + [pltpu.SemaphoreType.DMA((hops, experts))] * 2
        + [pltpu.SemaphoreType.DMA((2,))],
        compiler_params=pltpu.CompilerParams(collective_id=0, has_side_effects=True),
        name="dispatch",
    )(send, swished)


def combine_kernel(
    experts, parts, partial_ref, routed_ref, *rest
):
    bits = bits_of(parts)
    levels = len(bits)
    recv_bufs = rest[:levels]
    work, final = rest[levels], rest[levels + 1]
    hop_send, hop_recv, out_send, out_recv = rest[levels + 2 :]
    me, col = lax.axis_index("sp"), lax.axis_index("tp")
    width = routed_ref.shape[2]
    greet(
        [(lax.rem(me + k, experts), col) for k in range(1, experts)]
        + [(me, flipped(col, bit)) for bit in bits]
    )

    kept = [[col]]
    for bit in reversed(bits):
        kept.insert(0, kept[0] + [flipped(column, bit) for column in kept[0]])
    starts, total = [], 0
    for level in range(levels):
        starts.append(total)
        total += len(kept[level + 1])

    def columns(column):
        return pl.ds(pl.multiple_of(column * width, width), width)

    def hop(level, slot, block):
        column = flipped(kept[level + 1][slot], bits[level])
        index = starts[level] + slot
        if level == 0:
            src = partial_ref.at[block, :, columns(column)]
        else:
            src = work.at[level - 1, slot, block]
        return remote(
            src, recv_bufs[level].at[slot, block], hop_send.at[index, block],
            hop_recv.at[index, block], (me, flipped(col, bits[level])),
        )

    def summed(level, slot_column, slot_path, block):
        value = partial_ref[block, :, columns(slot_column)].astype(jnp.float32)
        for stage in range(level):
            value = value + recv_bufs[stage][slot_path[stage], block].astype(jnp.float32)
        return value

    def block_of(k):
        return lax.rem(me + k, experts)

    def start_first(k, carry):
        for slot in range(len(kept[1])):
            hop(0, slot, block_of(k)).start()
        return carry

    lax.fori_loop(1, experts + 1, start_first, 0)

    for level in range(1, levels):

        def middle(k, carry, level=level):
            block = block_of(k)
            for slot in range(len(kept[level])):
                hop(level - 1, slot, block).wait_recv()
            size = len(kept[level + 1])
            for slot in range(size):
                value = summed(
                    level, kept[level][size + slot], [size + slot] * level, block
                )
                work[level - 1, slot, block] = value.astype(jnp.bfloat16)
            for slot in range(size):
                hop(level, slot, block).start()
            return carry

        lax.fori_loop(1, experts + 1, middle, 0)

    def out_copy(block):
        return remote(
            final.at[block], routed_ref.at[me], out_send.at[block], out_recv.at[me], (block, col)
        )

    def last(k, carry):
        block = block_of(k)
        hop(levels - 1, 0, block).wait_recv()
        value = summed(levels, col, [0] * levels, block).astype(jnp.bfloat16)

        @pl.when(k < experts)
        def _():
            final[block] = value
            out_copy(block).start()

        @pl.when(k == experts)
        def _():
            routed_ref[me] = value

        return carry

    lax.fori_loop(1, experts + 1, last, 0)

    def finish(k, carry):
        block = block_of(k)
        for level in range(levels):
            for slot in range(len(kept[level + 1])):
                hop(level, slot, block).wait_send()

        @pl.when(k < experts)
        def _():
            out_copy(block).wait_send()
            remote(
                final.at[block], routed_ref.at[block], out_send.at[block],
                out_recv.at[block], (block, col),
            ).wait_recv()

        return carry

    lax.fori_loop(1, experts + 1, finish, 0)


def combine(partial, experts, parts):
    _, capacity, full = partial.shape
    width = full // parts
    levels = len(bits_of(parts))
    hops = parts - 1
    recv = [
        VMEM((parts >> (level + 1), experts, capacity, width), jnp.bfloat16)
        for level in range(levels)
    ]
    return pl.pallas_call(
        functools.partial(combine_kernel, experts, parts),
        out_shape=jax.ShapeDtypeStruct((experts, capacity, width), jnp.bfloat16),
        in_specs=[pl.BlockSpec(memory_space=VMEM)],
        out_specs=pl.BlockSpec(memory_space=VMEM),
        scratch_shapes=recv
        + [
            VMEM((max(levels - 1, 1), max(parts // 4, 1), experts, capacity, width), jnp.bfloat16),
            VMEM((experts, capacity, width), jnp.bfloat16),
            pltpu.SemaphoreType.DMA((hops, experts)),
            pltpu.SemaphoreType.DMA((hops, experts)),
            pltpu.SemaphoreType.DMA((experts,)),
            pltpu.SemaphoreType.DMA((experts,)),
        ],
        compiler_params=pltpu.CompilerParams(collective_id=1, has_side_effects=True),
        name="combine",
    )(partial)


def tail_kernel(
    experts, parts, stream_ref, conv_out_ref, mean_ref, rstd_ref, gain_ref, taps_ref, proj_ref,
    gathered_ref, conv_ref, proj_grad_ref,
    whole, arrived, extended, stats, grads, norms,
    hop_send, hop_recv, out_send, out_recv, stat_send, stat_recv, halo_sem, local_sem,
):
    me, col = lax.axis_index("sp"), lax.axis_index("tp")
    width, rows = stream_ref.shape
    full = width * parts
    block = full // experts
    bits = bits_of(parts)[::-1]
    tap_count = taps_ref.shape[0]
    halo = extended.shape[0] - rows
    greet(
        [(lax.rem(me + k, experts), col) for k in range(1, experts)]
        + [(me, lax.rem(col + k, parts)) for k in range(1, parts)]
    )

    def part(column):
        return whole.at[pl.ds(pl.multiple_of(column * width, width), width), :]

    own = pltpu.make_async_copy(stream_ref, part(col), local_sem.at[0])
    own.start()
    index, held, copies = 0, [col], []
    for level, bit in enumerate(bits):
        for slot, column in enumerate(held):
            src = stream_ref if column is col else part(column)
            copy = remote(
                src, part(column), hop_send.at[index + slot], hop_recv.at[index + slot],
                (me, flipped(col, bit)),
            )
            copy.start()
            copies.append(copy)
        for slot in range(len(held)):
            column = flipped(held[slot], bit)
            remote(
                part(column), part(column), hop_send.at[index + slot], hop_recv.at[index + slot],
                (me, flipped(col, bit)),
            ).wait_recv()
        index += len(held)
        held = held + [flipped(column, bit) for column in held]
    own.wait()

    def piece(peer):
        return whole.at[pl.ds(pl.multiple_of(peer * block, block), block), :]

    def landing(source):
        return arrived.at[:, pl.ds(pl.multiple_of(source * rows, rows), rows)]

    def out_copy(peer):
        return remote(piece(peer), landing(me), out_send.at[peer], out_recv.at[me], (peer, col))

    def start_out(k, carry):
        out_copy(lax.rem(me + k, experts)).start()
        return carry

    lax.fori_loop(1, experts, start_out, 0)
    mine = pltpu.make_async_copy(piece(me), landing(me), local_sem.at[1])
    mine.start()

    gain = gain_ref[...]
    rstd = rstd_ref[...]
    swished_grad = lax.dot_general(
        whole[...], proj_ref[...], OUTER_DIMS, preferred_element_type=jnp.float32
    )
    normed = (conv_out_ref[...].astype(jnp.float32) - mean_ref[...]) * rstd
    scaled = normed * gain
    sig = jax.nn.sigmoid(scaled)
    scaled_grad = swished_grad * sig * (1.0 + scaled * (1.0 - sig)) * gain
    grads[...] = scaled_grad
    norms[...] = normed
    first = jnp.sum(scaled_grad, axis=1, keepdims=True)
    second = jnp.sum(scaled_grad * normed, axis=1, keepdims=True)
    lane = lax.broadcasted_iota(jnp.int32, (rows, 128), 1)
    both = jnp.where(lane == 0, first, second)
    stats[parts] = both.T[:8]
    stat_copies = []
    for k in range(1, parts):
        copy = remote(
            stats.at[parts], stats.at[k], stat_send.at[k], stat_recv.at[k],
            (me, lax.rem(col + k, parts)),
        )
        copy.start()
        stat_copies.append(copy)
    for copy in stat_copies:
        copy.wait()
    total = stats[parts]
    for k in range(1, parts):
        total = total + stats[k]
    total = total / full
    spread = jnp.concatenate([total] * 16, axis=0).T
    first_mean = spread[:, 0:1]
    second_mean = spread[:, 1:2]
    extended[0:rows, :] = rstd * (grads[...] - first_mean - norms[...] * second_mean)

    def halo_copy(device):
        return remote(
            extended.at[pl.ds(0, halo), :], extended.at[pl.ds(rows, halo), :],
            halo_sem.at[0], halo_sem.at[1], (device, col),
        )

    @pl.when(me > 0)
    def _():
        halo_copy(lax.rem(me + experts - 1, experts)).start()

    @pl.when(me == experts - 1)
    def _():
        extended[rows:, :] = jnp.zeros((halo, width), jnp.float32)

    @pl.when(me < experts - 1)
    def _():
        halo_copy(lax.rem(me + experts - 1, experts)).wait_recv()

    for start in range(0, width, 128):
        cols = pl.ds(start, 128)
        total = jnp.zeros((rows, 128), jnp.float32)
        for offset in range(tap_count):
            total = total + taps_ref[offset : offset + 1, cols] * extended[pl.ds(offset, rows), cols]
        conv_ref[:, cols] = total.astype(jnp.bfloat16)

    def finish(k, carry):
        source = lax.rem(me - k + experts, experts)
        remote(
            piece(source), landing(source), out_send.at[source], out_recv.at[source], (source, col)
        ).wait_recv()
        out_copy(source).wait_send()
        return carry

    lax.fori_loop(1, experts, finish, 0)
    mine.wait()
    proj_grad_ref[...] = jnp.dot(
        arrived[...], gathered_ref[...], preferred_element_type=jnp.float32
    )
    for copy in copies:
        copy.wait_send()

    @pl.when(me > 0)
    def _():
        halo_copy(lax.rem(me + experts - 1, experts)).wait_send()


def tail(stream_t, conv_out, mean, rstd, gain, taps, proj, gathered, experts, parts):
    width, rows = stream_t.shape
    full = width * parts
    block = full // experts
    halo = -(-(taps.shape[0] - 1) // 8) * 8
    return pl.pallas_call(
        functools.partial(tail_kernel, experts, parts),
        out_shape=(
            jax.ShapeDtypeStruct((rows, width), jnp.bfloat16),
            jax.ShapeDtypeStruct((block, width), jnp.float32),
        ),
        in_specs=[pl.BlockSpec(memory_space=VMEM)] * 8,
        out_specs=[pl.BlockSpec(memory_space=VMEM)] * 2,
        scratch_shapes=[
            VMEM((full, rows), jnp.bfloat16),
            VMEM((block, experts * rows), jnp.bfloat16),
            VMEM((rows + halo, width), jnp.float32),
            VMEM((parts + 1, 8, rows), jnp.float32),
            VMEM((rows, width), jnp.float32),
            VMEM((rows, width), jnp.float32),
            pltpu.SemaphoreType.DMA((parts - 1,)),
            pltpu.SemaphoreType.DMA((parts - 1,)),
            pltpu.SemaphoreType.DMA((experts,)),
            pltpu.SemaphoreType.DMA((experts,)),
            pltpu.SemaphoreType.DMA((parts,)),
            pltpu.SemaphoreType.DMA((parts,)),
            pltpu.SemaphoreType.DMA((2,)),
            pltpu.SemaphoreType.DMA((2,)),
        ],
        compiler_params=pltpu.CompilerParams(collective_id=2, has_side_effects=True),
        name="tail",
    )(stream_t, conv_out, mean, rstd, gain, taps, proj, gathered)


def body(
    out_cotangent,
    expert_input,
    routes,
    route_weights,
    gate_proj,
    up_proj,
    down_proj,
    conv_out,
    conv_mean,
    conv_rstd,
    norm_gain,
    taps,
    out_proj,
):
    tok_rows, local_width = out_cotangent.shape
    experts = lax.axis_size("sp")
    parts = lax.axis_size("tp")
    capacity = 3 * tok_rows // experts
    full_width = local_width * parts
    slots = experts * capacity

    chosen = routes[:, :, None] == jnp.arange(experts, dtype=jnp.int32)[None, None, :]
    named = jnp.any(chosen, axis=1)
    weight = jnp.sum(jnp.where(chosen, route_weights[:, :, None], 0.0), axis=1)
    before = jnp.arange(tok_rows)[None, :] < jnp.arange(tok_rows)[:, None]
    rank = jnp.dot(
        before.astype(jnp.bfloat16), named.astype(jnp.bfloat16), preferred_element_type=jnp.float32
    ).astype(jnp.int32)
    rank = jnp.where(named, rank, -1)
    pick = rank.T[:, None, :] == jnp.arange(capacity, dtype=jnp.int32)[None, :, None]
    slot_weight = jnp.sum(jnp.where(pick, weight.T[:, None, :], 0.0), axis=2)
    pick = pick.astype(jnp.bfloat16).reshape(slots, tok_rows)
    send_rows = jnp.dot(pick, expert_input, preferred_element_type=jnp.float32).astype(jnp.bfloat16)
    send_cot = (
        jnp.dot(pick, out_cotangent, preferred_element_type=jnp.float32)
        * slot_weight.reshape(slots, 1)
    ).astype(jnp.bfloat16)
    send = jnp.stack(
        [send_rows.reshape(experts, capacity, local_width), send_cot.reshape(experts, capacity, local_width)],
        axis=1,
    )
    normed = (conv_out.astype(jnp.float32) - conv_mean[:, None]) * conv_rstd[:, None]
    scaled = normed * norm_gain[None, :]
    swished = (scaled * jax.nn.sigmoid(scaled)).astype(jnp.bfloat16)

    arrived, gathered = dispatch(send, swished, experts, parts)
    rows_in = arrived[0].reshape(slots, full_width)
    cot_in = arrived[1].reshape(slots, full_width)
    gate_local = gate_proj[0]
    up_local = up_proj[0]
    down_local = down_proj[0]
    gate_pre = jnp.dot(rows_in, gate_local, preferred_element_type=jnp.float32)
    up_pre = jnp.dot(rows_in, up_local, preferred_element_type=jnp.float32)
    gate_sigmoid = jax.nn.sigmoid(gate_pre)
    activation = (gate_pre * gate_sigmoid * up_pre).astype(jnp.bfloat16)
    act_grad = lax.dot_general(cot_in, down_local, INNER_DIMS, preferred_element_type=jnp.float32)
    gate_back = (act_grad * up_pre * gate_sigmoid * (1.0 + gate_pre * (1.0 - gate_sigmoid))).astype(
        jnp.bfloat16
    )
    up_back = (act_grad * gate_pre * gate_sigmoid).astype(jnp.bfloat16)
    down_grad = lax.dot_general(
        activation, cot_in, OUTER_DIMS, preferred_element_type=jnp.float32
    ).astype(jnp.bfloat16)[None]
    gate_grad = lax.dot_general(
        rows_in, gate_back, OUTER_DIMS, preferred_element_type=jnp.float32
    ).astype(jnp.bfloat16)[None]
    up_grad = lax.dot_general(
        rows_in, up_back, OUTER_DIMS, preferred_element_type=jnp.float32
    ).astype(jnp.bfloat16)[None]
    partial_rows = lax.dot_general(
        gate_back, gate_local, INNER_DIMS, preferred_element_type=jnp.float32
    )
    partial_rows = partial_rows + lax.dot_general(
        up_back, up_local, INNER_DIMS, preferred_element_type=jnp.float32
    )
    partial = partial_rows.astype(jnp.bfloat16).reshape(experts, capacity, full_width)
    routed = combine(partial, experts, parts).reshape(slots, local_width)
    routed_sum = lax.dot_general(pick, routed, OUTER_DIMS, preferred_element_type=jnp.float32)
    stream = (out_cotangent.astype(jnp.float32) + routed_sum).astype(jnp.bfloat16)
    conv_in_grad, proj_grad = tail(
        stream.T, conv_out, conv_mean[:, None], conv_rstd[:, None], norm_gain[None, :], taps,
        out_proj, gathered.reshape(experts * tok_rows, local_width), experts, parts,
    )
    return (gate_grad, up_grad, down_grad, proj_grad, stream, conv_in_grad)


def solution(mesh):
    in_specs = (
        P("sp", "tp"),
        P("sp", "tp"),
        P("sp", None),
        P("sp", None),
        P("sp", None, "tp"),
        P("sp", None, "tp"),
        P("sp", "tp", None),
        P("sp", "tp"),
        P("sp"),
        P("sp"),
        P("tp"),
        P(None, "tp"),
        P(None, "tp"),
    )
    out_specs = (
        P("sp", None, "tp"),
        P("sp", None, "tp"),
        P("sp", "tp", None),
        P("sp", "tp"),
        P("sp", "tp"),
        P("sp", "tp"),
    )
    return jax.shard_map(body, mesh=mesh, in_specs=in_specs, out_specs=out_specs, check_vma=False)
```

time: 219 us -> 138 us (0.63)
  the two profiles are of different devices: /device:TPU:0 before, /device:TPU:15 now
where the time goes in v1:
time: 138 us
  Pallas kernels  96.6 us (70%)
  matrix products  26.3 us (19%)
  local copies, waits for them, and re-layouts  9.68 us (7%)
  other arithmetic  4.41 us (3%)
    pallas_call x1, Pallas kernels, dispatch(): pl.pallas_call(functools.partial(dispatch_kernel, experts, parts), out_sh...  48.1 us
    pallas_call x1, Pallas kernels, tail(): pl.pallas_call(functools.partial(tail_kernel, experts, parts), out_shape=...  27.6 us
    pallas_call x1, Pallas kernels, combine(): pl.pallas_call(functools.partial(combine_kernel, experts, parts), out_sha...  20.9 us
    unnamed x18, local copies, waits for them, and re-layouts  4.39 us
    dot_general x1, matrix products, body(): lax.dot_general(rows_in, gate_back, OUTER_DIMS, preferred_element_type=jn...  4.11 us
    dot_general x1, matrix products, body(): lax.dot_general(rows_in, up_back, OUTER_DIMS, preferred_element_type=jnp....  4.11 us
    dot_general x1, matrix products, body(): lax.dot_general(activation, cot_in, OUTER_DIMS, preferred_element_type=jn...  3.99 us
    dot_general x1, matrix products, body(): lax.dot_general(up_back, up_local, INNER_DIMS, preferred_element_type=jnp...  3.07 us

profile of v1, /device:TPU:15, one launch (start us, length us, event | category | flops | bytes accessed | tf_op | source)
XLA Modules:
  0.0 137.8 jit_solution(14978916947682078514)
XLA Ops:
  0.6 0.0 copy-start
  0.6 0.7 fusion.18
  1.4 0.1 fusion.15
  1.5 0.7 select_reduce_fusion.1
  2.2 0.1 select_reduce_fusion
  2.4 0.1 mul.53
  2.4 0.1 eq.43
  2.5 0.1 bitcast_compare_fusion
  2.7 1.4 %copy.29.rstd_ref = f32[128,1]{1,0:T(8,128)} copy(f32[128,1]{0,1:T(1,128)} %bitcast.73) | data formatting | bytes 1024 | tf_op jit(solution)/shard_map/broadcast_in_dim | solution.py:538
  4.1 1.4 %copy.28.mean_ref = f32[128,1]{1,0:T(8,128)} copy(f32[128,1]{0,1:T(1,128)} %bitcast.74) | data formatting | bytes 1024 | tf_op jit(solution)/shard_map/broadcast_in_dim | solution.py:538
  5.4 1.0 copy.26
  6.5 1.8 %multiply_convert_fusion.4.swished_ref = bf16[128,512]{1,0:T(8,128)(2,1)} fusion(bf16[128,512]{1,0:T(8,128)(2,1)} %conv_out_ref.1, f32[512]{0:T(512)} %param.23, f32[128]{0:T(128)} %param.22, f32[128]{0:T(128)} %param.21), kind=kLoop, calls=%fused_computation.28 | loop fusion | flops 589824 | bytes 265216 | tf_op jit(solution)/shard_map/convert_element_type | solution.py:540
  8.2 1.2 fusion.12
  9.4 0.0 copy-done
  9.4 0.2 convolution_convert_fusion
  9.7 1.0 pad_maximum_fusion.send_ref
  10.6 48.1 %dispatch.1 = (bf16[2,8,48,2048]{3,2,1,0:T(8,128)(2,1)}, bf16[8,128,512]{2,1,0:T(8,128)(2,1)}) custom-call(bf16[8,2,48,512]{3,2,1,0:T(8,128)(2,1)} %pad_maximum_fusion.send_ref, bf16[128,512]{1,0:T(8,128)(2,1)} %multiply_convert_fusion.4.swished_ref), custom_call_target="tpu_custom_call" | custom-call | tf_op jit(solution)/shard_map/dispatch/pallas_call | solution.py:163
  58.7 0.0 copy-start.5
  58.7 2.3 %fusion.20 = (bf16[1,8,48,2048]{3,2,1,0:T(8,128)(2,1)S(1)}, bf16[1,8,48,2048]{3,2,1,0:T(8,128)(2,1)S(1)}) fusion(bf16[2,8,48,2048]{3,2,1,0:T(8,128)(2,1)} %get-tuple-element.10), kind=kLoop, calls=%fused_computation.38 | loop fusion | bytes 6291456 | tf_op jit(solution)/shard_map/slice | solution.py:544
  61.1 0.6 copy-done.5
  61.7 0.0 copy-start.6
  61.7 1.8 %fusion.2 = f32[384,896]{1,0:T(8,128)S(1)} fusion(bf16[384,2048]{1,0:T(8,128)(2,1)S(1)} %bitcast.62, bf16[1,2048,896]{2,1,0:T(8,128)(2,1)S(1)} %copy-done.5), kind=kOutput, calls=%fused_computation.2 | convolution fusion | flops 1409286144 | bytes 6619136 | tf_op jit(solution)/shard_map/dot_general | solution.py:548
  63.5 0.3 copy-done.6
  63.7 0.0 copy-start.4
  63.7 1.8 %fusion.6 = f32[384,896]{1,0:T(8,128)S(1)} fusion(bf16[384,2048]{1,0:T(8,128)(2,1)S(1)} %bitcast.63, bf16[1,2048,896]{2,1,0:T(8,128)(2,1)S(1)} %copy-done.6), kind=kOutput, calls=%fused_computation.6 | convolution fusion | flops 1409286144 | bytes 6619136 | tf_op jit(solution)/shard_map/dot_general | solution.py:549
  65.5 0.3 copy-done.4
  65.8 2.1 %multiply_convert_fusion.1 = (bf16[384,896]{1,0:T(8,128)(2,1)S(1)}, bf16[384,896]{1,0:T(8,128)(2,1)S(1)}) fusion(f32[384,896]{1,0:T(8,128)S(1)} %fusion.2, f32[384,896]{1,0:T(8,128)S(1)} %fusion.6, bf16[384,2048]{1,0:T(8,128)(2,1)S(1)} %bitcast.66, bf16[1,896,2048]{2,1,0:T(8,128)(2,1)S(1)} %copy-done.4), kind=kOutput, calls=%fused_computation.15 | convolution fusion | flops 1413758976 | bytes 9371648 | tf_op jit(solution)/shard_map/dot_general | solution.py:552
  67.9 4.0 %convert_bitcast_fusion = bf16[1,896,2048]{2,1,0:T(8,128)(2,1)} fusion(bf16[384,2048]{1,0:T(8,128)(2,1)S(1)} %bitcast.67, f32[384,896]{1,0:T(8,128)S(1)} %fusion.6, f32[384,896]{1,0:T(8,128)S(1)} %fusion.2), kind=kOutput, calls=%fused_computation.10 | convolution fusion | flops 1413185536 | bytes 7995392 | tf_op jit(solution)/shard_map/dot_general | solution.py:557
  71.9 1.9 %fusion = f32[384,2048]{1,0:T(8,128)S(1)} fusion(bf16[384,896]{1,0:T(8,128)(2,1)S(1)} %get-tuple-element.29, bf16[1,2048,896]{2,1,0:T(8,128)(2,1)S(1)} %copy-done.5), kind=kOutput, calls=%fused_computation | convolution fusion | flops 1409286144 | bytes 7503872 | tf_op jit(solution)/shard_map/dot_general | solution.py:566
  73.7 3.1 %add_convert_fusion = bf16[384,2048]{1,0:T(8,128)(2,1)} fusion(f32[384,2048]{1,0:T(8,128)S(1)} %fusion, bf16[384,896]{1,0:T(8,128)(2,1)S(1)} %get-tuple-element.28, bf16[1,2048,896]{2,1,0:T(8,128)(2,1)S(1)} %copy-done.6), kind=kOutput, calls=%fused_computation.13 | convolution fusion | flops 1410859008 | bytes 9076736 | tf_op jit(solution)/shard_map/dot_general | solution.py:569
  76.8 20.9 %combine.1 = bf16[8,48,512]{2,1,0:T(8,128)(2,1)} custom-call(bf16[8,48,2048]{2,1,0:T(8,128)(2,1)} %bitcast.68), custom_call_target="tpu_custom_call" | custom-call | tf_op jit(solution)/shard_map/combine/pallas_call | solution.py:302
  97.7 2.0 %fusion.14 = bf16[128,512]{0,1:T(8,128)(2,1)} fusion(bf16[8,48,512]{2,1,0:T(8,128)(2,1)} %combine.1, bf16[128,512]{0,1:T(8,128)(2,1)S(1)} %copy.26, s32[8,128]{1,0:T(8,128)S(1)} %fusion.15), kind=kOutput, calls=%fused_computation.23 | convolution fusion | flops 50577408 | bytes 659456 | tf_op jit(solution)/shard_map/dot_general | solution.py:574
  99.7 0.0 copy-start.1
  99.7 27.6 %tail.1 = (bf16[128,512]{1,0:T(8,128)(2,1)}, f32[256,512]{1,0:T(8,128)}) custom-call(bf16[512,128]{1,0:T(8,128)(2,1)} %bitcast.69, bf16[128,512]{1,0:T(8,128)(2,1)} %conv_out_ref.1, f32[128,1]{1,0:T(8,128)} %copy.28.mean_ref, f32[128,1]{1,0:T(8,128)} %copy.29.rstd_ref, f32[1,512]{1,0:T(1,128)} %bitcast.72, f32[31,512]{1,0:T(8,128)} %taps_ref.1, ...), custom_call_target="tpu_custom_call" | custom-call | tf_op jit(solution)/shard_map/tail/pallas_call | solution.py:467
  127.3 0.0 copy-done.1
  127.3 0.8 copy.30
  128.1 4.1 %convert_bitcast_fusion.1 = bf16[1,2048,896]{2,1,0:T(8,128)(2,1)} fusion(bf16[384,2048]{1,0:T(8,128)(2,1)S(1)} %bitcast.64, bf16[384,896]{1,0:T(8,128)(2,1)S(1)} %get-tuple-element.28), kind=kOutput, calls=%fused_computation.11 | convolution fusion | flops 1411121152 | bytes 5931008 | tf_op jit(solution)/shard_map/dot_general | solution.py:563
  132.2 0.0 copy-start.2
  132.2 0.0 copy-start.3
  132.2 4.1 %convert_bitcast_fusion.2 = bf16[1,2048,896]{2,1,0:T(8,128)(2,1)} fusion(bf16[384,2048]{1,0:T(8,128)(2,1)S(1)} %bitcast.65, bf16[384,896]{1,0:T(8,128)(2,1)S(1)} %get-tuple-element.29), kind=kOutput, calls=%fused_computation.12 | convolution fusion | flops 1411121152 | bytes 5931008 | tf_op jit(solution)/shard_map/dot_general | solution.py:560
  136.3 0.0 copy-done.2
  136.3 0.8 copy.38
  137.1 0.0 copy-done.3
  137.1 0.7 copy.39
  (1 shorter events, 0.0 us)
Async XLA Ops:
  0.6 8.8 %copy-start = (bf16[128,512]{1,0:T(8,128)(2,1)S(1)}, bf16[128,512]{1,0:T(8,128)(2,1)}, u32[]{:S(2)}) copy-start(bf16[128,512]{1,0:T(8,128)(2,1)} %param.14) | copy-start | bytes 393220
  58.7 3.0 %copy-start.5 = (bf16[1,2048,896]{2,1,0:T(8,128)(2,1)S(1)}, bf16[1,2048,896]{2,1,0:T(8,128)(2,1)}, u32[]{:S(2)}) copy-start(bf16[1,2048,896]{2,1,0:T(8,128)(2,1)} %param.17) | copy-start | bytes 11010052
  61.7 2.0 %copy-start.6 = (bf16[1,2048,896]{2,1,0:T(8,128)(2,1)S(1)}, bf16[1,2048,896]{2,1,0:T(8,128)(2,1)}, u32[]{:S(2)}) copy-start(bf16[1,2048,896]{2,1,0:T(8,128)(2,1)} %param.18) | copy-start | bytes 11010052
  63.7 2.0 %copy-start.4 = (bf16[1,896,2048]{2,1,0:T(8,128)(2,1)S(1)}, bf16[1,896,2048]{2,1,0:T(8,128)(2,1)}, u32[]{:S(2)}) copy-start(bf16[1,896,2048]{2,1,0:T(8,128)(2,1)} %param.19) | copy-start | bytes 11010052
  99.7 27.6 %copy-start.1 = (bf16[128,512]{0,1:T(8,128)(2,1)S(1)}, bf16[128,512]{0,1:T(8,128)(2,1)}, u32[]{:S(2)}) copy-start(bf16[128,512]{0,1:T(8,128)(2,1)} %fusion.14) | copy-start | bytes 393220
  132.2 4.1 %copy-start.2 = (f32[256,512]{1,0:T(8,128)S(1)}, f32[256,512]{1,0:T(8,128)}, u32[]{:S(2)}) copy-start(f32[256,512]{1,0:T(8,128)} %get-tuple-element.39) | copy-start | bytes 1572868
  132.2 4.9 %copy-start.3 = (bf16[128,512]{1,0:T(8,128)(2,1)S(1)}, bf16[128,512]{1,0:T(8,128)(2,1)}, u32[]{:S(2)}) copy-start(bf16[128,512]{1,0:T(8,128)(2,1)} %get-tuple-element.41) | copy-start | bytes 393220

commit v2 on v1

--- a/solution.py
+++ b/solution.py
@@ -40,42 +40,41 @@
 
 
 def dispatch_kernel(
-    experts, parts, send_ref, swished_ref, full_ref, gathered_ref,
-    out_send, out_recv, sw_send, sw_recv, hop_send, hop_recv, local_sem,
+    experts, parts, rows_send_ref, cot_send_ref, rows_ref, cot_ref,
+    out_send, out_recv, hop_send, hop_recv, local_sem,
 ):
     me, col = lax.axis_index("sp"), lax.axis_index("tp")
-    width = send_ref.shape[3]
+    width = rows_send_ref.shape[2]
     bits = bits_of(parts)[::-1]
     greet(
         [(lax.rem(me + k, experts), col) for k in range(1, experts)]
         + [(me, flipped(col, bit)) for bit in bits]
     )
-
-    def place(source, column):
-        return full_ref.at[:, source, :, pl.ds(pl.multiple_of(column * width, width), width)]
-
-    own = pltpu.make_async_copy(send_ref.at[me], place(me, col), local_sem.at[0])
-    own.start()
-    own_sw = pltpu.make_async_copy(swished_ref, gathered_ref.at[me], local_sem.at[1])
-    own_sw.start()
-
-    def out_copy(peer, slot):
-        return remote(send_ref.at[peer], place(me, col), out_send.at[peer], out_recv.at[me], (peer, col))
-
-    def sw_copy(peer):
-        return remote(swished_ref, gathered_ref.at[me], sw_send.at[peer], sw_recv.at[me], (peer, col))
-
-    def start_out(k, carry):
-        out_copy(lax.rem(me + k, experts), k).start()
-        return carry
-
-    def start_sw(k, carry):
-        sw_copy(lax.rem(me + k, experts)).start()
-        return carry
-
-    lax.fori_loop(1, experts, start_out, 0)
-    lax.fori_loop(1, experts, start_sw, 0)
-    own.wait()
+    sends, fulls = (rows_send_ref, cot_send_ref), (rows_ref, cot_ref)
+
+    def place(kind, source, column):
+        return fulls[kind].at[source, :, pl.ds(pl.multiple_of(column * width, width), width)]
+
+    def out_copy(kind, peer):
+        return remote(
+            sends[kind].at[peer], place(kind, me, col), out_send.at[kind, peer],
+            out_recv.at[kind, me], (peer, col),
+        )
+
+    own = []
+    for kind in range(2):
+        own.append(
+            pltpu.make_async_copy(sends[kind].at[me], place(kind, me, col), local_sem.at[kind])
+        )
+        own[kind].start()
+
+        def start_out(k, carry, kind=kind):
+            out_copy(kind, lax.rem(me + k, experts)).start()
+            return carry
+
+        lax.fori_loop(1, experts, start_out, 0)
+    for copy in own:
+        copy.wait()
 
     held = [[col]]
     for bit in bits:
@@ -85,111 +84,107 @@
         starts.append(total)
         total += len(held[level])
 
-    def hop(level, slot, column, source):
+    def hop(kind, level, slot, column, source):
         index = starts[level] + slot
         return remote(
-            place(source, column), place(source, column),
-            hop_send.at[index, source], hop_recv.at[index, source],
+            place(kind, source, column), place(kind, source, column),
+            hop_send.at[kind, index, source], hop_recv.at[kind, index, source],
             (me, flipped(col, bits[level])),
         )
 
-    def hop_arrival(level, slot, source):
-        index = starts[level] + slot
-        column = flipped(held[level][slot], bits[level])
-        return remote(
-            place(source, column), place(source, column),
-            hop_send.at[index, source], hop_recv.at[index, source],
-            (me, flipped(col, bits[level])),
-        )
-
-    def advance(k, carry):
-        source = lax.rem(me - k + experts, experts)
-
-        @pl.when((k > 0) & (k < experts))
-        def _():
-            remote(
-                send_ref.at[source], place(source, col), out_send.at[source],
-                out_recv.at[source], (source, col),
-            ).wait_recv()
-
-        @pl.when(k < experts)
-        def _():
+    def hop_arrival(kind, level, slot, source):
+        return hop(kind, level, slot, flipped(held[level][slot], bits[level]), source)
+
+    for kind in range(2):
+
+        def advance(k, carry, kind=kind):
+            source = lax.rem(me - k + experts, experts)
+
+            @pl.when((k > 0) & (k < experts))
+            def _():
+                remote(
+                    sends[kind].at[source], place(kind, source, col), out_send.at[kind, source],
+                    out_recv.at[kind, source], (source, col),
+                ).wait_recv()
+
+            @pl.when(k < experts)
+            def _():
+                for level in range(len(bits)):
+                    hop(kind, level, 0, col, source).start()
+
+            for level in range(1, len(bits)):
+                late = lax.rem(me - k + level + 2 * experts, experts)
+
+                @pl.when((k >= level) & (k < experts + level))
+                def _(level=level, late=late):
+                    size = len(held[level - 1])
+                    for slot in range(size):
+                        hop_arrival(kind, level - 1, slot, late).wait_recv()
+                    for later in range(level, len(bits)):
+                        for slot in range(size, 2 * size):
+                            hop(kind, later, slot, held[level][slot], late).start()
+
+            return carry
+
+        lax.fori_loop(0, experts + len(bits) - 1, advance, 0)
+
+    for kind in range(2):
+
+        def finish(k, carry, kind=kind):
+            source = lax.rem(me + k, experts)
+            last = len(bits) - 1
+            for slot in range(len(held[last])):
+                hop_arrival(kind, last, slot, source).wait_recv()
             for level in range(len(bits)):
-                hop(level, 0, col, source).start()
-
-        for level in range(1, len(bits)):
-            late = lax.rem(me - k + level + 2 * experts, experts)
-
-            @pl.when((k >= level) & (k < experts + level))
-            def _(level=level, late=late):
-                size = len(held[level - 1])
-                for slot in range(size):
-                    hop_arrival(level - 1, slot, late).wait_recv()
-                for later in range(level, len(bits)):
-                    for slot in range(size, 2 * size):
-                        hop(later, slot, held[level][slot], late).start()
-
-        return carry
-
-    lax.fori_loop(0, experts + len(bits) - 1, advance, 0)
-
-    def finish(k, carry):
-        source = lax.rem(me + k, experts)
-        last = len(bits) - 1
-        for slot in range(len(held[last])):
-            hop_arrival(last, slot, source).wait_recv()
-        for level in range(len(bits)):
-            for slot in range(len(held[level])):
-                hop(level, slot, held[level][slot], source).wait_send()
-
-        @pl.when(k > 0)
-        def _():
-            out_copy(source, k).wait_send()
-            sw_copy(source).wait_send()
-            remote(
-                swished_ref, gathered_ref.at[source], sw_send.at[source],
-                sw_recv.at[source], (source, col),
-            ).wait_recv()
-
-        return carry
-
-    lax.fori_loop(0, experts, finish, 0)
-    own_sw.wait()
-
-
-def dispatch(send, swished, experts, parts):
-    _, _, capacity, width = send.shape
+                for slot in range(len(held[level])):
+                    hop(kind, level, slot, held[level][slot], source).wait_send()
+
+            @pl.when(k > 0)
+            def _():
+                out_copy(kind, source).wait_send()
+
+            return carry
+
+        lax.fori_loop(0, experts, finish, 0)
+
+
+def dispatch(rows_send, cot_send, experts, parts):
+    _, capacity, width = rows_send.shape
     hops = parts - 1
+    full = jax.ShapeDtypeStruct((experts, capacity, width * parts), jnp.bfloat16)
     return pl.pallas_call(
         functools.partial(dispatch_kernel, experts, parts),
-        out_shape=(
-            jax.ShapeDtypeStruct((2, experts, capacity, width * parts), jnp.bfloat16),
-            jax.ShapeDtypeStruct((experts,) + swished.shape, jnp.bfloat16),
-        ),
+        out_shape=(full, full),
         in_specs=[pl.BlockSpec(memory_space=VMEM)] * 2,
         out_specs=[pl.BlockSpec(memory_space=VMEM)] * 2,
-        scratch_shapes=[pltpu.SemaphoreType.DMA((experts,))] * 4
-        + [pltpu.SemaphoreType.DMA((hops, experts))] * 2
+        scratch_shapes=[pltpu.SemaphoreType.DMA((2, experts))] * 2
+        + [pltpu.SemaphoreType.DMA((2, hops, experts))] * 2
         + [pltpu.SemaphoreType.DMA((2,))],
         compiler_params=pltpu.CompilerParams(collective_id=0, has_side_effects=True),
         name="dispatch",
-    )(send, swished)
+    )(rows_send, cot_send)
+
+
+def column_of(row, rows):
+    return jnp.broadcast_to(row, (128, rows)).T[:, 0:1]
 
 
 def combine_kernel(
-    experts, parts, partial_ref, routed_ref, *rest
+    experts, parts, partial_ref, conv_out_ref, mean_ref, rstd_ref, gain_ref, routed_ref, near_ref,
+    *rest,
 ):
     bits = bits_of(parts)
     levels = len(bits)
     recv_bufs = rest[:levels]
     work, final = rest[levels], rest[levels + 1]
-    hop_send, hop_recv, out_send, out_recv = rest[levels + 2 :]
+    hop_send, hop_recv, out_send, out_recv, sw_send, sw_recv = rest[levels + 2 :]
     me, col = lax.axis_index("sp"), lax.axis_index("tp")
     width = routed_ref.shape[2]
     greet(
         [(lax.rem(me + k, experts), col) for k in range(1, experts)]
         + [(me, flipped(col, bit)) for bit in bits]
     )
+    tokens = conv_out_ref.shape[0]
 
     kept = [[col]]
     for bit in reversed(bits):
@@ -229,6 +224,33 @@
         return carry
 
     lax.fori_loop(1, experts + 1, start_first, 0)
+
+    scaled = (
+        (conv_out_ref[...].astype(jnp.float32) - column_of(mean_ref[...], tokens))
+        * column_of(rstd_ref[...], tokens)
+        * gain_ref[...]
+    )
+    near_ref[me // 2] = (scaled * jax.nn.sigmoid(scaled)).astype(jnp.bfloat16)
+
+    far_bits = bits_of(experts)[:0:-1]
+    sources = [[me]]
+    for bit in far_bits:
+        sources.append(sources[-1] + [flipped(source, bit) for source in sources[-1]])
+
+    def sw_copy(level, slot, source):
+        index = (1 << level) - 1 + slot
+        return remote(
+            near_ref.at[source // 2], near_ref.at[source // 2], sw_send.at[index],
+            sw_recv.at[index], (flipped(me, far_bits[level]), col),
+        )
+
+    def sw_start(level):
+        for slot, source in enumerate(sources[level]):
+            sw_copy(level, slot, source).start()
+
+    def sw_arrive(level):
+        for slot, source in enumerate(sources[level]):
+            sw_copy(level, slot, flipped(source, far_bits[level])).wait_recv()
 
     for level in range(1, levels):
 
@@ -248,6 +270,8 @@
 
         lax.fori_loop(1, experts + 1, middle, 0)
 
+    sw_start(0)
+
     def out_copy(block):
         return remote(
             final.at[block], routed_ref.at[me], out_send.at[block], out_recv.at[me], (block, col)
@@ -270,6 +294,10 @@
         return carry
 
     lax.fori_loop(1, experts + 1, last, 0)
+    for level in range(len(far_bits)):
+        sw_arrive(level)
+        if level + 1 < len(far_bits):
+            sw_start(level + 1)
 
     def finish(k, carry):
         block = block_of(k)
@@ -288,9 +316,12 @@
         return carry
 
     lax.fori_loop(1, experts + 1, finish, 0)
-
-
-def combine(partial, experts, parts):
+    for level in range(len(far_bits)):
+        for slot, source in enumerate(sources[level]):
+            sw_copy(level, slot, source).wait_send()
+
+
+def combine(partial, conv_out, mean, rstd, gain, experts, parts):
     _, capacity, full = partial.shape
     width = full // parts
     levels = len(bits_of(parts))
@@ -301,9 +332,12 @@
     ]
     return pl.pallas_call(
         functools.partial(combine_kernel, experts, parts),
-        out_shape=jax.ShapeDtypeStruct((experts, capacity, width), jnp.bfloat16),
-        in_specs=[pl.BlockSpec(memory_space=VMEM)],
-        out_specs=pl.BlockSpec(memory_space=VMEM),
+        out_shape=(
+            jax.ShapeDtypeStruct((experts, capacity, width), jnp.bfloat16),
+            jax.ShapeDtypeStruct((experts // 2,) + conv_out.shape, jnp.bfloat16),
+        ),
+        in_specs=[pl.BlockSpec(memory_space=VMEM)] * 5,
+        out_specs=[pl.BlockSpec(memory_space=VMEM)] * 2,
         scratch_shapes=recv
         + [
             VMEM((max(levels - 1, 1), max(parts // 4, 1), experts, capacity, width), jnp.bfloat16),
@@ -312,17 +346,19 @@
             pltpu.SemaphoreType.DMA((hops, experts)),
             pltpu.SemaphoreType.DMA((experts,)),
             pltpu.SemaphoreType.DMA((experts,)),
+            pltpu.SemaphoreType.DMA((experts // 2,)),
+            pltpu.SemaphoreType.DMA((experts // 2,)),
         ],
         compiler_params=pltpu.CompilerParams(collective_id=1, has_side_effects=True),
         name="combine",
-    )(partial)
+    )(partial, conv_out, mean, rstd, gain)
 
 
 def tail_kernel(
     experts, parts, stream_ref, conv_out_ref, mean_ref, rstd_ref, gain_ref, taps_ref, proj_ref,
-    gathered_ref, conv_ref, proj_grad_ref,
-    whole, arrived, extended, stats, grads, norms,
-    hop_send, hop_recv, out_send, out_recv, stat_send, stat_recv, halo_sem, local_sem,
+    near_ref, conv_ref, proj_grad_ref,
+    whole, arrived, far, extended, stats, grads, norms,
+    hop_send, hop_recv, out_send, out_recv, stat_send, stat_recv, halo_sem, local_sem, far_sem,
 ):
     me, col = lax.axis_index("sp"), lax.axis_index("tp")
     width, rows = stream_ref.shape
@@ -335,6 +371,9 @@
         [(lax.rem(me + k, experts), col) for k in range(1, experts)]
         + [(me, lax.rem(col + k, parts)) for k in range(1, parts)]
     )
+
+    far_copy = remote(near_ref, far, far_sem.at[0], far_sem.at[1], (flipped(me, 1), col))
+    far_copy.start()
 
     def part(column):
         return whole.at[pl.ds(pl.multiple_of(column * width, width), width), :]
@@ -364,26 +403,27 @@
     def piece(peer):
         return whole.at[pl.ds(pl.multiple_of(peer * block, block), block), :]
 
-    def landing(source):
-        return arrived.at[:, pl.ds(pl.multiple_of(source * rows, rows), rows)]
+    def landing(receiver, source):
+        slot = lax.rem(receiver + source, 2) * (experts // 2) + source // 2
+        return arrived.at[:, pl.ds(pl.multiple_of(slot * rows, rows), rows)]
 
     def out_copy(peer):
-        return remote(piece(peer), landing(me), out_send.at[peer], out_recv.at[me], (peer, col))
+        return remote(piece(peer), landing(peer, me), out_send.at[peer], out_recv.at[me], (peer, col))
 
     def start_out(k, carry):
         out_copy(lax.rem(me + k, experts)).start()
         return carry
 
     lax.fori_loop(1, experts, start_out, 0)
-    mine = pltpu.make_async_copy(piece(me), landing(me), local_sem.at[1])
+    mine = pltpu.make_async_copy(piece(me), landing(me, me), local_sem.at[1])
     mine.start()
 
     gain = gain_ref[...]
-    rstd = rstd_ref[...]
+    rstd = column_of(rstd_ref[...], rows)
     swished_grad = lax.dot_general(
         whole[...], proj_ref[...], OUTER_DIMS, preferred_element_type=jnp.float32
     )
-    normed = (conv_out_ref[...].astype(jnp.float32) - mean_ref[...]) * rstd
+    normed = (conv_out_ref[...].astype(jnp.float32) - column_of(mean_ref[...], rows)) * rstd
     scaled = normed * gain
     sig = jax.nn.sigmoid(scaled)
     scaled_grad = swished_grad * sig * (1.0 + scaled * (1.0 - sig)) * gain
@@ -441,15 +481,20 @@
     def finish(k, carry):
         source = lax.rem(me - k + experts, experts)
         remote(
-            piece(source), landing(source), out_send.at[source], out_recv.at[source], (source, col)
+            piece(source), landing(me, source), out_send.at[source], out_recv.at[source], (source, col)
         ).wait_recv()
         out_copy(source).wait_send()
         return carry
 
     lax.fori_loop(1, experts, finish, 0)
     mine.wait()
+    half = experts // 2 * rows
     proj_grad_ref[...] = jnp.dot(
-        arrived[...], gathered_ref[...], preferred_element_type=jnp.float32
+        arrived[:, :half], near_ref[...].reshape(half, width), preferred_element_type=jnp.float32
+    )
+    far_copy.wait()
+    proj_grad_ref[...] += jnp.dot(
+        arrived[:, half:], far[...].reshape(half, width), preferred_element_type=jnp.float32
     )
     for copy in copies:
         copy.wait_send()
@@ -459,7 +504,7 @@
         halo_copy(lax.rem(me + experts - 1, experts)).wait_send()
 
 
-def tail(stream_t, conv_out, mean, rstd, gain, taps, proj, gathered, experts, parts):
+def tail(stream_t, conv_out, mean, rstd, gain, taps, proj, near, experts, parts):
     width, rows = stream_t.shape
     full = width * parts
     block = full // experts
@@ -475,6 +520,7 @@
         scratch_shapes=[
             VMEM((full, rows), jnp.bfloat16),
             VMEM((block, experts * rows), jnp.bfloat16),
+            VMEM(near.shape, jnp.bfloat16),
             VMEM((rows + halo, width), jnp.float32),
             VMEM((parts + 1, 8, rows), jnp.float32),
             VMEM((rows, width), jnp.float32),
@@ -487,10 +533,11 @@
             pltpu.SemaphoreType.DMA((parts,)),
             pltpu.SemaphoreType.DMA((2,)),
             pltpu.SemaphoreType.DMA((2,)),
+            pltpu.SemaphoreType.DMA((2,)),
         ],
         compiler_params=pltpu.CompilerParams(collective_id=2, has_side_effects=True),
         name="tail",
-    )(stream_t, conv_out, mean, rstd, gain, taps, proj, gathered)
+    )(stream_t, conv_out, mean, rstd, gain, taps, proj, near)
 
 
 def body(
@@ -531,17 +578,14 @@
         jnp.dot(pick, out_cotangent, preferred_element_type=jnp.float32)
         * slot_weight.reshape(slots, 1)
     ).astype(jnp.bfloat16)
-    send = jnp.stack(
-        [send_rows.reshape(experts, capacity, local_width), send_cot.reshape(experts, capacity, local_width)],
-        axis=1,
-    )
-    normed = (conv_out.astype(jnp.float32) - conv_mean[:, None]) * conv_rstd[:, None]
-    scaled = normed * norm_gain[None, :]
-    swished = (scaled * jax.nn.sigmoid(scaled)).astype(jnp.bfloat16)
-
-    arrived, gathered = dispatch(send, swished, experts, parts)
-    rows_in = arrived[0].reshape(slots, full_width)
-    cot_in = arrived[1].reshape(slots, full_width)
+    arrived_rows, arrived_cot = dispatch(
+        send_rows.reshape(experts, capacity, local_width),
+        send_cot.reshape(experts, capacity, local_width),
+        experts, parts,
+    )
+    rows_in = arrived_rows.reshape(slots, full_width)
+    cot_in = arrived_cot.reshape(slots, full_width)
+    mean, rstd, gain = conv_mean[None, :], conv_rstd[None, :], norm_gain[None, :]
     gate_local = gate_proj[0]
     up_local = up_proj[0]
     down_local = down_proj[0]
@@ -570,12 +614,12 @@
         up_back, up_local, INNER_DIMS, preferred_element_type=jnp.float32
     )
     partial = partial_rows.astype(jnp.bfloat16).reshape(experts, capacity, full_width)
-    routed = combine(partial, experts, parts).reshape(slots, local_width)
+    routed, near = combine(partial, conv_out, mean, rstd, gain, experts, parts)
+    routed = routed.reshape(slots, local_width)
     routed_sum = lax.dot_general(pick, routed, OUTER_DIMS, preferred_element_type=jnp.float32)
     stream = (out_cotangent.astype(jnp.float32) + routed_sum).astype(jnp.bfloat16)
     conv_in_grad, proj_grad = tail(
-        stream.T, conv_out, conv_mean[:, None], conv_rstd[:, None], norm_gain[None, :], taps,
-        out_proj, gathered.reshape(experts * tok_rows, local_width), experts, parts,
+        stream.T, conv_out, mean, rstd, gain, taps, out_proj, near, experts, parts
     )
     return (gate_grad, up_grad, down_grad, proj_grad, stream, conv_in_grad)
 

time: 138 us -> 137 us (level)
  the two profiles are of different devices: /device:TPU:15 before, /device:TPU:0 now
where the time goes in v2:
time: 137 us
  Pallas kernels  101 us (74%)
  matrix products  29.7 us (22%)
  local copies, waits for them, and re-layouts  4.16 us (3%)
  other arithmetic  1.7 us (1%)
    pallas_call x1, Pallas kernels, dispatch(): pl.pallas_call(functools.partial(dispatch_kernel, experts, parts), out_sh...  41.7 us
    pallas_call x1, Pallas kernels, combine(): pl.pallas_call(functools.partial(combine_kernel, experts, parts), out_sha...  33.3 us
    pallas_call x1, Pallas kernels, tail(): pl.pallas_call(functools.partial(tail_kernel, experts, parts), out_shape=...  25.7 us
    dot_general x1, matrix products, body(): gate_pre = jnp.dot(rows_in, gate_local, preferred_element_type=jnp.float32)  4.44 us
    dot_general x1, matrix products, body(): lax.dot_general(rows_in, up_back, OUTER_DIMS, preferred_element_type=jnp....  4.11 us
    dot_general x1, matrix products, body(): lax.dot_general(rows_in, gate_back, OUTER_DIMS, preferred_element_type=jn...  4.1 us
    dot_general x1, matrix products, body(): lax.dot_general(activation, cot_in, OUTER_DIMS, preferred_element_type=jn...  4 us
    unnamed x22, local copies, waits for them, and re-layouts  3.99 us

profile of v2, /device:TPU:0, one launch (start us, length us, event | category | flops | bytes accessed | tf_op | source)
XLA Modules:
  0.0 137.1 jit_solution(16188065015692381339)
XLA Ops:
  0.6 0.0 copy-start
  0.6 0.7 fusion.18
  1.4 0.1 fusion.15
  1.5 0.7 select_reduce_fusion.1
  2.2 0.1 select_reduce_fusion
  2.4 0.1 mul.34
  2.4 0.1 eq.43
  2.5 0.1 bitcast_compare_fusion
  2.7 1.0 copy.24
  3.7 1.9 %fusion.12 = bf16[384,512]{1,0:T(8,128)(2,1)} fusion(pred[384,128]{1,0:T(32,128)(4,1)S(1)} %bitcast_compare_fusion, bf16[128,512]{1,0:T(8,128)(2,1)} %param.13, f32[384]{0:T(512)S(1)} %mul.34), kind=kOutput, calls=%fused_computation.19 | convolution fusion | flops 50724864 | bytes 574976 | tf_op jit(solution)/shard_map/dot_general | solution.py:578
  5.6 0.0 copy-done
  5.6 1.0 convolution_convert_fusion
  6.6 41.7 %dispatch.1 = (bf16[8,48,2048]{2,1,0:T(8,128)(2,1)}, bf16[8,48,2048]{2,1,0:T(8,128)(2,1)}) custom-call(bf16[8,48,512]{2,1,0:T(8,128)(2,1)} %bitcast.61, bf16[8,48,512]{2,1,0:T(8,128)(2,1)} %bitcast.60), custom_call_target="tpu_custom_call" | custom-call | tf_op jit(solution)/shard_map/dispatch/pallas_call | solution.py:155
  48.4 0.0 copy-start.6
  48.4 0.0 copy-start.7
  48.4 4.4 %fusion.2 = f32[384,896]{1,0:T(8,128)S(1)} fusion(bf16[384,2048]{1,0:T(8,128)(2,1)} %bitcast.70, bf16[1,2048,896]{2,1,0:T(8,128)(2,1)} %param.17), kind=kOutput, calls=%fused_computation.2 | convolution fusion | flops 1409286144 | bytes 6619136 | tf_op jit(solution)/shard_map/dot_general | solution.py:592
  52.8 0.0 copy-done.6
  52.8 0.0 copy-done.7
  52.8 0.0 copy-start.4
  52.9 0.0 copy-start.8
  52.9 1.8 %fusion.6 = f32[384,896]{1,0:T(8,128)S(1)} fusion(bf16[384,2048]{1,0:T(8,128)(2,1)S(1)} %bitcast.71, bf16[1,2048,896]{2,1,0:T(8,128)(2,1)S(1)} %copy-done.6), kind=kOutput, calls=%fused_computation.6 | convolution fusion | flops 1409286144 | bytes 6619136 | tf_op jit(solution)/shard_map/dot_general | solution.py:593
  54.7 0.2 copy-done.4
  54.9 0.5 copy-done.8
  55.4 2.1 %multiply_convert_fusion.1 = (bf16[384,896]{1,0:T(8,128)(2,1)S(1)}, bf16[384,896]{1,0:T(8,128)(2,1)S(1)}) fusion(f32[384,896]{1,0:T(8,128)S(1)} %fusion.2, f32[384,896]{1,0:T(8,128)S(1)} %fusion.6, bf16[384,2048]{1,0:T(8,128)(2,1)S(1)} %bitcast.74, bf16[1,896,2048]{2,1,0:T(8,128)(2,1)S(1)} %copy-done.4), kind=kOutput, calls=%fused_computation.15 | convolution fusion | flops 1413758976 | bytes 9371648 | tf_op jit(solution)/shard_map/dot_general | solution.py:596
  57.5 0.0 copy-start.5
  57.5 4.0 %convert_bitcast_fusion = bf16[1,896,2048]{2,1,0:T(8,128)(2,1)} fusion(bf16[384,2048]{1,0:T(8,128)(2,1)S(1)} %bitcast.75, f32[384,896]{1,0:T(8,128)S(1)} %fusion.6, f32[384,896]{1,0:T(8,128)S(1)} %fusion.2), kind=kOutput, calls=%fused_computation.10 | convolution fusion | flops 1413185536 | bytes 7995392 | tf_op jit(solution)/shard_map/dot_general | solution.py:601
  61.5 0.0 copy-done.5
  61.5 1.8 %fusion = f32[384,2048]{1,0:T(8,128)S(1)} fusion(bf16[384,896]{1,0:T(8,128)(2,1)S(1)} %get-tuple-element.31, bf16[1,2048,896]{2,1,0:T(8,128)(2,1)S(1)} %copy-done.5), kind=kOutput, calls=%fused_computation | convolution fusion | flops 1409286144 | bytes 7503872 | tf_op jit(solution)/shard_map/dot_general | solution.py:610
  63.4 3.0 %add_convert_fusion = bf16[384,2048]{1,0:T(8,128)(2,1)} fusion(f32[384,2048]{1,0:T(8,128)S(1)} %fusion, bf16[384,896]{1,0:T(8,128)(2,1)S(1)} %get-tuple-element.30, bf16[1,2048,896]{2,1,0:T(8,128)(2,1)S(1)} %copy-done.6), kind=kOutput, calls=%fused_computation.13 | convolution fusion | flops 1410859008 | bytes 9076736 | tf_op jit(solution)/shard_map/dot_general | solution.py:613
  66.3 33.3 %combine.1 = (bf16[8,48,512]{2,1,0:T(8,128)(2,1)}, bf16[4,128,512]{2,1,0:T(8,128)(2,1)}) custom-call(bf16[8,48,2048]{2,1,0:T(8,128)(2,1)} %bitcast.59, bf16[128,512]{1,0:T(8,128)(2,1)} %conv_out_ref.3, f32[1,128]{1,0:T(1,128)} %bitcast.66, f32[1,128]{1,0:T(1,128)} %bitcast.68, f32[1,512]{1,0:T(1,128)} %bitcast.64), custom_call_target="tpu_custom_call" | custom-call | tf_op jit(solution)/shard_map/combine/pallas_call | solution.py:333
  99.6 1.3 fusion.14
  100.9 0.0 copy-start.1
  100.9 0.8 copy.26
  101.7 0.0 copy-done.1
  101.7 25.7 %tail.1 = (bf16[128,512]{1,0:T(8,128)(2,1)}, f32[256,512]{1,0:T(8,128)}) custom-call(bf16[512,128]{1,0:T(8,128)(2,1)} %bitcast.62, bf16[128,512]{1,0:T(8,128)(2,1)} %conv_out_ref.3, f32[1,128]{1,0:T(1,128)} %bitcast.67, f32[1,128]{1,0:T(1,128)} %bitcast.69, f32[1,512]{1,0:T(1,128)} %bitcast.65, f32[31,512]{1,0:T(8,128)} %taps_ref.1, ...), custom_call_target="tpu_custom_call" | custom-call | tf_op jit(solution)/shard_map/tail/pallas_call | solution.py:512
  127.4 4.1 %convert_bitcast_fusion.1 = bf16[1,2048,896]{2,1,0:T(8,128)(2,1)} fusion(bf16[384,2048]{1,0:T(8,128)(2,1)S(1)} %bitcast.72, bf16[384,896]{1,0:T(8,128)(2,1)S(1)} %get-tuple-element.30), kind=kOutput, calls=%fused_computation.11 | convolution fusion | flops 1411121152 | bytes 5931008 | tf_op jit(solution)/shard_map/dot_general | solution.py:607
  131.5 0.0 copy-start.2
  131.5 0.0 copy-start.3
  131.5 4.1 %convert_bitcast_fusion.2 = bf16[1,2048,896]{2,1,0:T(8,128)(2,1)} fusion(bf16[384,2048]{1,0:T(8,128)(2,1)S(1)} %bitcast.73, bf16[384,896]{1,0:T(8,128)(2,1)S(1)} %get-tuple-element.31), kind=kOutput, calls=%fused_computation.12 | convolution fusion | flops 1411121152 | bytes 5931008 | tf_op jit(solution)/shard_map/dot_general | solution.py:604
  135.6 0.0 copy-done.2
  135.6 0.8 copy.34
  136.4 0.0 copy-done.3
  136.4 0.7 copy.35
  (1 shorter events, 0.0 us)
Async XLA Ops:
  0.6 5.0 %copy-start = (bf16[128,512]{1,0:T(8,128)(2,1)S(1)}, bf16[128,512]{1,0:T(8,128)(2,1)}, u32[]{:S(2)}) copy-start(bf16[128,512]{1,0:T(8,128)(2,1)} %param.14) | copy-start | bytes 393220
  48.4 4.5 %copy-start.6 = (bf16[1,2048,896]{2,1,0:T(8,128)(2,1)S(1)}, bf16[1,2048,896]{2,1,0:T(8,128)(2,1)}, u32[]{:S(2)}) copy-start(bf16[1,2048,896]{2,1,0:T(8,128)(2,1)} %param.18) | copy-start | bytes 11010052
  48.4 4.5 %copy-start.7 = (bf16[8,48,2048]{2,1,0:T(8,128)(2,1)S(1)}, bf16[8,48,2048]{2,1,0:T(8,128)(2,1)}, u32[]{:S(2)}) copy-start(bf16[8,48,2048]{2,1,0:T(8,128)(2,1)} %get-tuple-element.12) | copy-start | bytes 4718596
  52.8 2.0 %copy-start.4 = (bf16[1,896,2048]{2,1,0:T(8,128)(2,1)S(1)}, bf16[1,896,2048]{2,1,0:T(8,128)(2,1)}, u32[]{:S(2)}) copy-start(bf16[1,896,2048]{2,1,0:T(8,128)(2,1)} %param.19) | copy-start | bytes 11010052
  52.9 2.5 %copy-start.8 = (bf16[8,48,2048]{2,1,0:T(8,128)(2,1)S(1)}, bf16[8,48,2048]{2,1,0:T(8,128)(2,1)}, u32[]{:S(2)}) copy-start(bf16[8,48,2048]{2,1,0:T(8,128)(2,1)} %get-tuple-element.13) | copy-start | bytes 4718596
  57.5 4.0 %copy-start.5 = (bf16[1,2048,896]{2,1,0:T(8,128)(2,1)S(1)}, bf16[1,2048,896]{2,1,0:T(8,128)(2,1)}, u32[]{:S(2)}) copy-start(bf16[1,2048,896]{2,1,0:T(8,128)(2,1)} %param.17) | copy-start | bytes 11010052
  100.9 0.8 copy-start.1
  131.5 4.1 %copy-start.2 = (f32[256,512]{1,0:T(8,128)S(1)}, f32[256,512]{1,0:T(8,128)}, u32[]{:S(2)}) copy-start(f32[256,512]{1,0:T(8,128)} %get-tuple-element.41) | copy-start | bytes 1572868
  131.5 4.9 %copy-start.3 = (bf16[128,512]{1,0:T(8,128)(2,1)S(1)}, bf16[128,512]{1,0:T(8,128)(2,1)}, u32[]{:S(2)}) copy-start(bf16[128,512]{1,0:T(8,128)(2,1)} %get-tuple-element.43) | copy-start | bytes 393220
